TPU v7x, 256 devices: a whole 4x4x8 slice. The times are simulated.
256 devices in a mesh: ep: 32 (over z, x), tp: 8 (over y, core).
Axes of the slice: x: 4, y: 4, z: 8, core: 2. Of those that a mesh axis runs over, the one named last changes fastest.
Arguments:
- queries: bfloat16 [16384, 1024], P('ep', 'tp'), may hold values from -8 to 8
- keys_values: bfloat16 [16384, 1024], P('ep', 'tp'), may hold values from -60 to 60
- forget_cache: float32 [16, 16384], P('tp'), may hold values from -2460 to 0, as said below
- heads_gain: float32 [1024], replicated, may hold values from 0.1 to 1.9
- output_weight: bfloat16 [1024, 2048], replicated, may hold values from -0.1875 to 0.1875
- expert_tokens: bfloat16 [4096, 2048], P('ep'), may hold values from -600 to 600
- expert_gain: float32 [2048], replicated, may hold values from 0.1 to 1.9
- routes: int32 [4096, 4], P('ep'), may hold values from 0 to 31, all different within a row; in each aligned block of 128 rows (0 to 127, 128 to 255, ...) at most 32 rows name the same one
- route_logits: float32 [4096, 4], P('ep'), may hold values from -6 to 301
- gate_weight: bfloat16 [32, 2048, 2048], P('ep', None, 'tp'), may hold values from -0.5 to 0.5
- up_weight: bfloat16 [32, 2048, 2048], P('ep', None, 'tp'), may hold values from -0.5 to 0.5
- down_weight: bfloat16 [32, 2048, 2048], P('ep', 'tp'), may hold values from -0.015625 to 0.015625
Outputs:
- mixer_out: bfloat16 [16384, 2048], P(('ep', 'tp'))
- moe_out: bfloat16 [4096, 2048], P('ep', 'tp')
Inputs may be any that keep to these rules, and one draw needn't show every extreme that they name: `forget_cache`: each row never rises from one position to the next. `routes`: the 4 experts of a row differ. In each aligned block of 128 rows (one device's tokens) no expert is named more than 32 times, so slot is below 32; some expert is named exactly 32 times in some block.
All inputs are finite; a program needn't handle non-finite values.
Results may differ from a plain program's by a relative error of at most 0.017.
Values may be sent and summed in bfloat16 or wider, within the bound.
A program may use at most 128 MiB of HBM per device.

v0:
```python
import math
import jax
import jax.numpy as jnp
from jax import lax
from jax.sharding import Mesh
from jax.sharding import PartitionSpec as P

HEAD = 64
EP = ("ep_0", "ep_1")
EP_TP = ("ep_0", "ep_1", "tp")
epsilon = 1e-06
clamp_limit = 7.0
sigmoid_slope = 1.702


def gathered_by_axis(array, axes, dim):
    whole = array
    for number in range(len(axes) - 1, -1, -1):
        whole = lax.all_gather(whole, axes[number], axis=dim, tiled=True)
    return whole


def in_blocks(array, dim, devices):
    before, after = (array.shape[:dim], array.shape[dim + 1 :])
    return jnp.moveaxis(array.reshape(*before, devices, -1, *after), dim, 0)


def sent_and_summed(array, axis, dim):
    devices = lax.axis_size(axis)
    parts = lax.all_to_all(in_blocks(array, dim, devices), axis, 0, 0, tiled=True)
    return jnp.sum(parts.astype(jnp.float32), axis=0)


def scaled_rows(values, gain_vector):
    as_float = values.astype(jnp.float32)
    inverse = lax.rsqrt(jnp.mean(as_float * as_float, axis=-1, keepdims=True) + epsilon)
    return (as_float * inverse * gain_vector).astype(jnp.bfloat16)


def assign_slots(routes, experts, capacity):
    row_count, pick_count = routes.shape
    flat_routes = routes.reshape(-1)
    onehot = (flat_routes[:, None] == jnp.arange(experts, dtype=jnp.int32)[None, :]).astype(
        jnp.int32
    )
    earlier = jnp.cumsum(onehot, axis=0) - onehot
    slot_rank = jnp.sum(earlier * onehot, axis=1)
    position = flat_routes * capacity + slot_rank
    owner_row = jnp.arange(row_count * pick_count, dtype=jnp.int32) // pick_count
    slot_token = jnp.full((experts * capacity,), row_count, jnp.int32).at[position].set(owner_row)
    return (position.reshape(row_count, pick_count), slot_token)


def body(
    queries,
    keys_values,
    forget_cache,
    heads_gain,
    output_weight,
    expert_tokens,
    expert_gain,
    routes,
    route_logits,
    gate_weight,
    up_weight,
    down_weight,
):
    row_count = queries.shape[0]
    query_count = queries.shape[1] // HEAD
    key_count = keys_values.shape[1] // (2 * HEAD)
    group_size = query_count // key_count
    offset = lax.axis_index(EP) * row_count
    score_scale = 1.0 / math.sqrt(HEAD)
    count_rows = queries.shape[0]
    segment_positions = offset + jnp.arange(count_rows, dtype=jnp.int32)
    gate_rows = lax.dynamic_slice_in_dim(forget_cache, offset, count_rows, 1)
    segment_bias = gate_rows.T.reshape(count_rows, key_count, group_size, 1)
    segments = [
        (queries.reshape(count_rows, key_count, group_size, HEAD), segment_positions, segment_bias)
    ]
    start_states = tuple(
        [
            (
                jnp.full((grouped.shape[0], key_count, group_size), -jnp.inf, jnp.float32),
                jnp.zeros((grouped.shape[0], key_count, group_size), jnp.float32),
                jnp.zeros((grouped.shape[0], key_count, group_size, HEAD), jnp.float32),
            )
            for grouped, positions, bias in segments
        ]
    )
    piece_rows = gathered_by_axis(keys_values.reshape(row_count, key_count, 2 * HEAD), EP, 0)
    count_rows = piece_rows.shape[0]
    block_width = 512
    blocks = piece_rows.reshape(count_rows // block_width, block_width, key_count, 2 * HEAD)

    def one_block(states, scan_item):
        block_rows, block_index = scan_item
        first_key = block_index * block_width
        key_block = block_rows[:, :, :HEAD]
        value_block = block_rows[:, :, HEAD:]
        key_gate = lax.dynamic_slice_in_dim(forget_cache, first_key, block_width, 1).reshape(
            1, key_count, group_size, block_width
        )
        key_pos = first_key + jnp.arange(block_width, dtype=jnp.int32)
        updated = []
        for (grouped, positions, bias), state in zip(segments, states):

            def take_block(state_in, grouped=grouped, positions=positions, bias=bias):
                running_max, running_sum, weighted = state_in
                scores = (
                    jnp.einsum(
                        "qhgd,khd->qhgk", grouped, key_block, preferred_element_type=jnp.float32
                    )
                    * score_scale
                )
                scores = scores + bias - key_gate
                visible = (key_pos[None, :] <= positions[:, None])[:, None, None, :]
                scores = jnp.where(visible, scores, -jnp.inf)
                new_max = jnp.maximum(running_max, jnp.max(scores, axis=-1))
                safe_max = jnp.where(jnp.isfinite(new_max), new_max, 0.0)
                factor = jnp.exp(running_max - safe_max)
                weights = jnp.exp(scores - safe_max[..., None])
                running_sum = running_sum * factor + jnp.sum(weights, axis=-1)
                weighted = weighted * factor[..., None] + jnp.einsum(
                    "qhgk,khd->qhgd",
                    weights.astype(jnp.bfloat16),
                    value_block,
                    preferred_element_type=jnp.float32,
                )
                return (new_max, running_sum, weighted)

            def keep_state(state_in):
                return state_in

            updated.append(lax.cond(first_key <= positions[-1], take_block, keep_state, state))
        return (tuple(updated), None)

    final_states, _ = lax.scan(
        one_block, start_states, (blocks, jnp.arange(count_rows // block_width, dtype=jnp.int32))
    )
    outputs = [
        (weighted / running_sum[..., None])
        .reshape(running_sum.shape[0], query_count * HEAD)
        .astype(jnp.bfloat16)
        for running_max, running_sum, weighted in final_states
    ]
    attended = outputs[0]
    local_rows = lax.all_to_all(attended, "tp", split_axis=0, concat_axis=1, tiled=True)
    heads_normed = scaled_rows(local_rows, heads_gain)
    mixer_out = jnp.dot(heads_normed, output_weight, preferred_element_type=jnp.float32).astype(
        jnp.bfloat16
    )
    experts_count = lax.axis_size(EP)
    expert_rows, pick_count = routes.shape
    capacity = 2 * expert_rows * pick_count // experts_count
    expert_in = scaled_rows(expert_tokens, expert_gain)
    shifted = route_logits - jnp.max(route_logits, axis=1, keepdims=True)
    raised = jnp.exp(shifted)
    route_weight = raised / jnp.sum(raised, axis=1, keepdims=True)
    position, slot_token = assign_slots(routes, experts_count, capacity)
    model_width = expert_in.shape[1]
    part_width = model_width // lax.axis_size("tp")
    gate_local = gate_weight[0]
    up_local = up_weight[0]
    down_local = down_weight[0]
    own_columns = lax.dynamic_slice_in_dim(
        expert_in, lax.axis_index("tp") * part_width, part_width, 1
    )
    padded = jnp.concatenate([own_columns, jnp.zeros((1, part_width), jnp.bfloat16)], axis=0)
    outgoing = jnp.take(padded, slot_token, axis=0).reshape(experts_count, capacity, part_width)
    arrived = lax.all_to_all(outgoing, EP, split_axis=0, concat_axis=0, tiled=True).reshape(
        experts_count * capacity, part_width
    )
    piece_rows = lax.all_gather(arrived, "tp", axis=1, tiled=True)
    gate_sum = jnp.dot(piece_rows, gate_local, preferred_element_type=jnp.float32)
    up_sum = jnp.dot(piece_rows, up_local, preferred_element_type=jnp.float32)
    gate_cut = jnp.minimum(gate_sum, clamp_limit)
    up_cut = jnp.clip(up_sum, -clamp_limit, clamp_limit)
    hidden = ((up_cut + 1.0) * gate_cut * jax.nn.sigmoid(sigmoid_slope * gate_cut)).astype(
        jnp.bfloat16
    )
    expert_out = sent_and_summed(
        lax.dot_general(
            down_local, hidden, (((0,), (1,)), ((), ())), preferred_element_type=jnp.float32
        ).astype(jnp.bfloat16),
        "tp",
        0,
    ).astype(jnp.bfloat16)
    returned = lax.all_to_all(expert_out, EP, split_axis=1, concat_axis=1, tiled=True)
    picked = jnp.take(returned, position.reshape(-1), axis=1).reshape(
        part_width, expert_rows, pick_count
    )
    moe_out = jnp.einsum("crk,rk->rc", picked.astype(jnp.float32), route_weight).astype(
        jnp.bfloat16
    )
    return (mixer_out, moe_out)


def solution(mesh):
    torus = Mesh(mesh.devices.reshape(8, 4, mesh.shape["tp"]), ("ep_0", "ep_1", "tp"))
    return jax.shard_map(
        body,
        mesh=torus,
        in_specs=(
            P(EP, "tp"),
            P(EP, "tp"),
            P("tp", None),
            P(),
            P(),
            P(EP, None),
            P(),
            P(EP, None),
            P(EP, None),
            P(EP, None, "tp"),
            P(EP, None, "tp"),
            P(EP, "tp", None),
        ),
        out_specs=(P(EP_TP, None), P(EP, "tp")),
        check_vma=False,
    )
```

profile of v0, /device:TPU:2, one launch (start us, length us, event | category | flops | bytes accessed | tf_op | source)
XLA Modules:
  0.0 385.4 jit_solution(9211881118816011675)
XLA Ops:
  7.2 1.2 convert_element_type.73
  8.4 1.2 multiply_reduce_fusion
  9.7 0.8 copy.40
  11.4 1.2 reduce-window.6
  13.2 2.4 scatter_custom_fusion
  15.7 0.8 dynamic-slice
  16.6 3.9 %gather_fusion = bf16[1024,256]{1,0:T(8,128)(2,1)S(1)} fusion(bf16[129,256]{1,0:T(8,128)(2,1)S(1)} %concatenate.3, s32[1024]{0:T(1024)S(1)} %fusion.43), kind=kCustom, calls=%fused_computation | custom fusion | bytes 1052672 | tf_op jit(solution)/shard_map/jit(_take)/gather | solution.py:170
  20.8 28.3 %all_to_all.32 = bf16[32,32,256]{2,1,0:T(8,128)(2,1)} all-to-all(bf16[32,32,256]{2,1,0:T(8,128)(2,1)S(1)} %broadcast_select_fusion), channel_id=1, replica_groups=mesh['ep_0'=8,'ep_1'=4,'tp'=8] {'ep_0','ep_1'}, dimensions={0} | all-to-all | bytes 1048576 | tf_op jit(solution)/shard_map/all_to_all | solution.py:171
  49.2 13.8 %all-gather = bf16[2048,128]{1,0:T(8,128)(2,1)} all-gather(bf16[512,128]{1,0:T(8,128)(2,1)S(1)} %copy-done.1), channel_id=2, replica_groups=mesh['ep_0'=8,'ep_1'=4,'tp'=8] {'ep_1'}, dimensions={0}, use_global_device_ids=true | all-gather | bytes 655360 | tf_op jit(solution)/shard_map/all_gather | solution.py:19
  63.1 21.2 %all-gather.5.cloned.1.call-done = bf16[1024,2048]{1,0:T(8,128)(2,1)} async-done(((bf16[1024,256]{1,0:T(8,128)(2,1)}), bf16[1024,2048]{1,0:T(8,128)(2,1)}) %all-gather.5.cloned.1.call-update) | async-done | bytes 4194320 | tf_op jit(solution)/shard_map/all_gather | solution.py:174
  84.3 4.5 %convolution_minimum_fusion = f32[1024,256]{1,0:T(8,128)} fusion(bf16[1024,2048]{1,0:T(8,128)(2,1)} %all-gather.5.cloned.1.call-done, bf16[1,2048,256]{2,1,0:T(8,128)(2,1)S(1)} %copy-done.6), kind=kOutput, calls=%fused_computation.29 | convolution fusion | flops 1074003968 | bytes 6291456 | tf_op jit(solution)/shard_map/dot_general | solution.py:175
  88.8 8.8 %convolution_convert_fusion = bf16[1024,2048]{1,0:T(8,128)(2,1)} fusion(f32[1024,256]{1,0:T(8,128)} %convolution_minimum_fusion, bf16[1024,2048]{1,0:T(8,128)(2,1)} %all-gather.5.cloned.1.call-done, bf16[1,256,2048]{2,1,0:T(8,128)(2,1)S(1)} %copy-done, bf16[1,2048,256]{2,1,0:T(8,128)(2,1)S(1)} %copy-done.7), kind=kOutput, calls=%fused_computation.27 | convolution fusion | flops 2151940096 | bytes 11534336 | tf_op jit(solution)/shard_map/dot_general | solution.py:183
  97.7 4.6 %copy.58 = bf16[128,8,8,256]{3,2,0,1:T(8,128)(2,1)} copy(bf16[128,8,8,256]{3,2,1,0:T(8,128)(2,1)} %bitcast.128) | data formatting | bytes 8388608 | tf_op jit(solution)/shard_map/reshape | solution.py:25
  102.3 4.7 %all-to-all-start.2 = ((bf16[8,256,1024]{1,2,0:T(8,128)(2,1)}), bf16[8,256,1024]{1,2,0:T(8,128)(2,1)}, u32[]{:S(2)}, u32[]{:S(2)}) async-start(bf16[8,256,1024]{1,2,0:T(8,128)(2,1)} %bitcast.125), calls=%async_computation.2 | async-start | bytes 8388608 | tf_op jit(solution)/shard_map/all_to_all | solution.py:30
  108.0 33.8 %all-gather.7.cloned.1.call-done = bf16[16384,128]{1,0:T(8,128)(2,1)} async-done(((bf16[2048,128]{1,0:T(8,128)(2,1)}), bf16[16384,128]{1,0:T(8,128)(2,1)}) %all-gather.7.cloned.1.call-update) | async-done | bytes 4194320 | tf_op jit(solution)/shard_map/all_gather | solution.py:19
  141.8 6.5 %copy.37 = bf16[32,512,1,128]{1,3,2,0:T(8,128)(2,1)} copy(bf16[32,512,1,128]{3,1,0,2:T(8,128)(2,1)} %bitcast.127) | data formatting | bytes 8388608 | tf_op jit(solution)/shard_map/while | solution.py:138
  148.4 87.1 %while.14 = (s32[]{:T(128)}, f32[512,1,2]{0,2,1:T(2,128)S(1)}, f32[512,1,2]{0,2,1:T(2,128)S(1)}, f32[512,1,2,64]{0,3,2,1:T(8,128)S(1)}, s32[32]{0:T(128)S(1)}, /...) while((s32[]{:T(128)}, f32[512,1,2]{0,2,1:T(2,128)S(1)}, ...), condition=%wide.region_5.6_spmd, body=%wide.region_0.5_spmd.sunk | while | flops 139339264 | bytes 7965025 | solution.py:138
  150.9 3.6 conditional.2
  150.9 0.8 constant_dynamic-slice_fusion
  151.9 0.9 dynamic-slice_bitcast_fusion
  152.8 0.7 fusion.55
  156.9 3.6 conditional.2
  156.9 0.8 constant_dynamic-slice_fusion
  157.9 0.9 dynamic-slice_bitcast_fusion
  235.8 0.8 copy.38
  236.6 4.3 %all-to-all-start = ((bf16[8,64,128]{2,1,0:T(8,128)(2,1)}), bf16[8,64,128]{2,1,0:T(8,128)(2,1)S(1)}, u32[]{:S(2)}, u32[]{:S(2)}) async-start(bf16[8,64,128]{2,1,0:T(8,128)(2,1)} %copy.38), calls=%async_computation | async-start | bytes 262144 | tf_op jit(solution)/shard_map/all_to_all | solution.py:148
  241.1 3.7 reduce_sum.68
  244.8 2.2 all-to-all-done
  247.0 111.8 %all-to-all-start.3 = ((bf16[256,32,32]{0,2,1:T(8,128)(2,1)}), bf16[256,32,32]{0,2,1:T(8,128)(2,1)S(1)}, u32[]{:S(2)}, u32[]{:S(2)}) async-start(bf16[256,32,32]{0,2,1:T(8,128)(2,1)} %bitcast.33), calls=%async_computation.3 | async-start | bytes 1048576 | tf_op jit(solution)/shard_map/all_to_all | solution.py:189
  359.2 3.8 convolution_convert_fusion.1
  363.0 12.5 %all-to-all-done.3 = bf16[256,32,32]{0,2,1:T(8,128)(2,1)S(1)} async-done(((bf16[256,32,32]{0,2,1:T(8,128)(2,1)}), bf16[256,32,32]{0,2,1:T(8,128)(2,1)S(1)}, u32[]{:S(2)}, u32[]{:S(2)}) %all-to-all-start.3) | async-done | bytes 524320 | tf_op jit(solution)/shard_map/all_to_all | solution.py:189
  375.5 1.9 gather_fusion.1
  (206 shorter events, 45.8 us)
Async XLA Ops:
  7.2 81.7 %copy-start = (bf16[1,256,2048]{2,1,0:T(8,128)(2,1)S(1)}, bf16[1,256,2048]{2,1,0:T(8,128)(2,1)}, u32[]{:S(2)}) copy-start(bf16[1,256,2048]{2,1,0:T(8,128)(2,1)} %param.27) | copy-start | bytes 3145732
  7.2 77.1 %all-gather.5.cloned.1.call-start = ((), (), s32[]{:S(2)}) async-start(), calls=%async_computation.4 | async-start | bytes 4718592 | tf_op jit(solution)/shard_map/all_gather | solution.py:174
  10.5 38.8 %copy-start.1 = (bf16[512,128]{1,0:T(8,128)(2,1)S(1)}, bf16[512,128]{1,0:T(8,128)(2,1)}, u32[]{:S(2)}) copy-start(bf16[512,128]{1,0:T(8,128)(2,1)} %param.17) | copy-start | bytes 393220
  16.6 67.7 %copy-start.6 = (bf16[1,2048,256]{2,1,0:T(8,128)(2,1)S(1)}, bf16[1,2048,256]{2,1,0:T(8,128)(2,1)}, u32[]{:S(2)}) copy-start(bf16[1,2048,256]{2,1,0:T(8,128)(2,1)} %param.25) | copy-start | bytes 3145732
  49.2 39.7 %copy-start.7 = (bf16[1,2048,256]{2,1,0:T(8,128)(2,1)S(1)}, bf16[1,2048,256]{2,1,0:T(8,128)(2,1)}, u32[]{:S(2)}) copy-start(bf16[1,2048,256]{2,1,0:T(8,128)(2,1)} %param.26) | copy-start | bytes 3145732
  49.2 92.7 %all-gather.7.cloned.1.call-start = ((), (), s32[]{:S(2)}) async-start(), calls=%async_computation.5 | async-start | bytes 4718592 | tf_op jit(solution)/shard_map/all_gather | solution.py:19
  102.3 4.8 %copy-start.2 = (bf16[512,128]{1,0:T(8,128)(2,1)S(1)}, bf16[512,128]{1,0:T(8,128)(2,1)}, u32[]{:S(2)}) copy-start(bf16[512,128]{1,0:T(8,128)(2,1)} %param.16) | copy-start | bytes 393220
  102.3 134.3 %all-to-all-start.2 = ((bf16[8,256,1024]{1,2,0:T(8,128)(2,1)}), bf16[8,256,1024]{1,2,0:T(8,128)(2,1)}, u32[]{:S(2)}, u32[]{:S(2)}) async-start(bf16[8,256,1024]{1,2,0:T(8,128)(2,1)} %bitcast.125), calls=%async_computation.2 | async-start | bytes 8388608 | tf_op jit(solution)/shard_map/all_to_all | solution.py:30
  148.4 92.5 %copy-start.3 = (s32[128,4]{0,1:T(4,128)S(1)}, s32[128,4]{0,1:T(4,128)}, u32[]{:S(2)}) copy-start(s32[128,4]{0,1:T(4,128)} %param.23) | copy-start | bytes 6148
  148.4 92.7 %copy-start.4 = (f32[128,4]{0,1:T(4,128)S(1)}, f32[128,4]{0,1:T(4,128)}, u32[]{:S(2)}) copy-start(f32[128,4]{0,1:T(4,128)} %param.24) | copy-start | bytes 6148
  235.5 123.6 %copy-start.5 = (f32[1024]{0:T(1024)S(1)}, f32[1024]{0:T(1024)}, u32[]{:S(2)}) copy-start(f32[1024]{0:T(1024)} %param.19) | copy-start | bytes 12292
  236.6 10.4 %all-to-all-start = ((bf16[8,64,128]{2,1,0:T(8,128)(2,1)}), bf16[8,64,128]{2,1,0:T(8,128)(2,1)S(1)}, u32[]{:S(2)}, u32[]{:S(2)}) async-start(bf16[8,64,128]{2,1,0:T(8,128)(2,1)} %copy.38), calls=%async_computation | async-start | bytes 262144 | tf_op jit(solution)/shard_map/all_to_all | solution.py:148
  247.0 128.5 %all-to-all-start.3 = ((bf16[256,32,32]{0,2,1:T(8,128)(2,1)}), bf16[256,32,32]{0,2,1:T(8,128)(2,1)S(1)}, u32[]{:S(2)}, u32[]{:S(2)}) async-start(bf16[256,32,32]{0,2,1:T(8,128)(2,1)} %bitcast.33), calls=%async_computation.3 | async-start | bytes 1048576 | tf_op jit(solution)/shard_map/all_to_all | solution.py:189
Sparse Core Ops, SparseCore 0:
  49.3 34.9 all-gather.4
  86.1 55.6 all-gather.6
where the time goes:
time: 388 us; the launch traced here: 385 us
  starting transfers between devices  121 us (31%)
  waiting for transfers between devices  69.8 us (18%)
  local copies, waits for them, and re-layouts  65.9 us (17%)
  loops' own time  42.4 us (11%)
  blocking collectives  42.2 us (11%)
  matrix products  20 us (5%)
  between operations  14.3 us (4%)
  other arithmetic  9.81 us (3%)
    all_to_all x1, starting transfers between devices, body(): lax.all_to_all(expert_out, EP, split_axis=1, concat_axis=1, tiled=True)  112 us
    another operation x1, loops' own time, body(): lax.scan(one_block, start_states, (blocks, jnp.arange(count_rows // block...  41.9 us
    all_gather x1, waiting for transfers between devices, gathered_by_axis(): whole = lax.all_gather(whole, axes[number], axis=dim, tiled=True)  33.8 us
    all_to_all x1, blocking collectives, body(): lax.all_to_all(outgoing, EP, split_axis=0, concat_axis=0, tiled=True)  28.3 us
    all_gather x1, waiting for transfers between devices, body(): piece_rows = lax.all_gather(arrived, 'tp', axis=1, tiled=True)  21.2 us
    slice x32, local copies, waits for them, and re-layouts, one_block(): positions[-1]  18.9 us
    dynamic_slice x32, local copies, waits for them, and re-layouts, body(): lax.scan(one_block, start_states, (blocks, jnp.arange(count_rows // block...  18.8 us
    all_gather x1, blocking collectives, gathered_by_axis(): whole = lax.all_gather(whole, axes[number], axis=dim, tiled=True)  13.8 us
  transfers between devices with their start and end apart: 5, of which 4 were waited for; matrix products, arithmetic and copies ran while one was open for 21% of the time, Pallas kernels for 0%

commit v1 on v0

--- a/solution.py
+++ b/solution.py
@@ -11,6 +11,35 @@
 epsilon = 1e-06
 clamp_limit = 7.0
 sigmoid_slope = 1.702
+
+
+def _remake_zone(sheet):
+    parts_out, frame_out, placed = (lax.axis_size("tp"), lax.axis_index("tp"), sheet.shape[1])
+    part_next = lax.dynamic_update_slice_in_dim(
+        jnp.zeros(
+            [tick * parts_out if m == 1 else tick for m, tick in enumerate(sheet.shape)],
+            sheet.dtype,
+        ),
+        sheet,
+        frame_out * placed,
+        axis=1,
+    )
+    field_out = wide_out = sheet
+    for j0 in range(1, parts_out // 2 + 1):
+        field_out = lax.ppermute(
+            field_out, "tp", [(m, (m + 1) % parts_out) for m in range(parts_out)]
+        )
+        part_next = lax.dynamic_update_slice_in_dim(
+            part_next, field_out, (frame_out - j0) % parts_out * placed, axis=1
+        )
+        if 2 * j0 < parts_out:
+            wide_out = lax.ppermute(
+                wide_out, "tp", [(m, (m - 1) % parts_out) for m in range(parts_out)]
+            )
+            part_next = lax.dynamic_update_slice_in_dim(
+                part_next, wide_out, (frame_out + j0) % parts_out * placed, axis=1
+            )
+    return part_next
 
 
 def gathered_by_axis(array, axes, dim):
@@ -171,7 +200,7 @@
     arrived = lax.all_to_all(outgoing, EP, split_axis=0, concat_axis=0, tiled=True).reshape(
         experts_count * capacity, part_width
     )
-    piece_rows = lax.all_gather(arrived, "tp", axis=1, tiled=True)
+    piece_rows = _remake_zone(arrived)
     gate_sum = jnp.dot(piece_rows, gate_local, preferred_element_type=jnp.float32)
     up_sum = jnp.dot(piece_rows, up_local, preferred_element_type=jnp.float32)
     gate_cut = jnp.minimum(gate_sum, clamp_limit)

time: 388 us -> 357 us (0.920)
  blocking collectives: 42.2 us -> 15.8 us
  waiting for transfers between devices: 69.8 us -> 44.2 us
  starting transfers between devices: 121 us -> 142 us
    all_gather x1, waiting for transfers between devices: 33.8 us -> 0.01 us  [gathered_by_axis(): whole = lax.all_gather(whole, axes[number], axis=dim, tiled=True)]
    ppermute x0 -> x7, waiting for transfers between devices: none -> 28.6 us  [the longest x4 28.6 us: _remake_zone(): lax.ppermute(field_out, 'tp', [(m, (m + 1) % parts_out) for m in range(pa...]
    all_to_all x1 -> x0, blocking collectives: 28.3 us -> none  [body(): lax.all_to_all(outgoing, EP, split_axis=0, concat_axis=0, tiled=True)]
    all_gather x1 -> x0, waiting for transfers between devices: 21.2 us -> none  [body(): piece_rows = lax.all_gather(arrived, 'tp', axis=1, tiled=True)]
    all_to_all x0 -> x1, starting transfers between devices: none -> 11.6 us  [body(): lax.all_to_all(outgoing, EP, split_axis=0, concat_axis=0, tiled=True)]
    ppermute x0 -> x7, starting transfers between devices: none -> 8.88 us  [the longest x3 8.87 us: _remake_zone(): lax.ppermute(wide_out, 'tp', [(m, (m - 1) % parts_out) for m in range(par...]
  transfers between devices with their start and end apart: 5 -> 12, of which waited for: 4 -> 7; matrix products, arithmetic and copies ran while one was open for 21% -> 22% of each run, Pallas kernels for 0% -> 0%
where the time goes in v1:
time: 357 us; the launch traced here: 354 us
  starting transfers between devices  142 us (40%)
  local copies, waits for them, and re-layouts  69.3 us (19%)
  waiting for transfers between devices  44.2 us (12%)
  loops' own time  40.6 us (11%)
  matrix products  16.5 us (5%)
  blocking collectives  15.8 us (4%)
  between operations  14.5 us (4%)
  other arithmetic  10.6 us (3%)
    all_to_all x1, starting transfers between devices, body(): lax.all_to_all(expert_out, EP, split_axis=1, concat_axis=1, tiled=True)  112 us
    another operation x1, loops' own time, body(): lax.scan(one_block, start_states, (blocks, jnp.arange(count_rows // block...  40 us
    ppermute x4, waiting for transfers between devices, _remake_zone(): lax.ppermute(field_out, 'tp', [(m, (m + 1) % parts_out) for m in range(pa...  28.6 us
    dynamic_slice x32, local copies, waits for them, and re-layouts, body(): lax.scan(one_block, start_states, (blocks, jnp.arange(count_rows // block...  18.8 us
    slice x32, local copies, waits for them, and re-layouts, one_block(): positions[-1]  18.4 us
    all_gather x1, blocking collectives, gathered_by_axis(): whole = lax.all_gather(whole, axes[number], axis=dim, tiled=True)  15.8 us
    all_to_all x1, waiting for transfers between devices, body(): lax.all_to_all(expert_out, EP, split_axis=1, concat_axis=1, tiled=True)  12.5 us
    all_to_all x1, starting transfers between devices, body(): lax.all_to_all(outgoing, EP, split_axis=0, concat_axis=0, tiled=True)  11.6 us
  transfers between devices with their start and end apart: 12, of which 7 were waited for; matrix products, arithmetic and copies ran while one was open for 22% of the time, Pallas kernels for 0%

profile of v1, /device:TPU:2, one launch (start us, length us, event | category | flops | bytes accessed | tf_op | source)
XLA Modules:
  0.0 353.8 jit_solution(8555545510241620625)
XLA Ops:
  7.2 1.2 convert_element_type.73
  8.4 1.3 multiply_reduce_fusion
  11.4 1.2 reduce-window.6
  13.2 2.4 scatter_custom_fusion
  16.6 3.9 %gather_fusion = bf16[1024,256]{1,0:T(8,128)(2,1)S(1)} fusion(bf16[129,256]{1,0:T(8,128)(2,1)S(1)} %concatenate.3, s32[1024]{0:T(1024)S(1)} %fusion.43), kind=kCustom, calls=%fused_computation | custom fusion | bytes 1052672 | tf_op jit(solution)/shard_map/jit(_take)/gather | solution.py:199
  20.6 1.0 broadcast_select_fusion
  21.6 11.6 %all-to-all-start.1 = ((bf16[32,32,256]{2,1,0:T(8,128)(2,1)}), bf16[32,32,256]{2,1,0:T(8,128)(2,1)S(1)}, u32[]{:S(2)}, u32[]{:S(2)}) async-start(bf16[32,32,256]{2,1,0:T(8,128)(2,1)} %broadcast_select_fusion), calls=%async_computation.1 | async-start | bytes 1048576 | tf_op jit(solution)/shard_map/all_to_all | solution.py:200
  33.3 15.8 %all-gather = bf16[2048,128]{1,0:T(8,128)(2,1)} all-gather(bf16[512,128]{1,0:T(8,128)(2,1)S(1)} %copy-done.4), channel_id=2, replica_groups=mesh['ep_0'=8,'ep_1'=4,'tp'=8] {'ep_1'}, dimensions={0}, use_global_device_ids=true | all-gather | bytes 655360 | tf_op jit(solution)/shard_map/all_gather | solution.py:48
  50.0 3.0 collective-permute-start.1
  53.0 6.9 %collective-permute-done = bf16[1024,256]{1,0:T(8,128)(2,1)S(1)} collective-permute-done((bf16[1024,256]{1,0:T(8,128)(2,1)S(1)}, bf16[1024,256]{1,0:T(8,128)(2,1)S(1)}, u32[]{:S(2)}, u32[]{:S(2)}) %collective-permute-start) | collective-permute-done | bytes 524320 | tf_op jit(solution)/shard_map/ppermute | solution.py:29
  59.9 3.0 collective-permute-start.3
  62.8 7.0 %collective-permute-done.2 = bf16[1024,256]{1,0:T(8,128)(2,1)} collective-permute-done((bf16[1024,256]{1,0:T(8,128)(2,1)S(1)}, bf16[1024,256]{1,0:T(8,128)(2,1)}, u32[]{:S(2)}, u32[]{:S(2)}) %collective-permute-start.2) | collective-permute-done | bytes 524320 | tf_op jit(solution)/shard_map/ppermute | solution.py:29
  70.4 3.0 collective-permute-start.5
  73.4 6.4 %collective-permute-done.4 = bf16[1024,256]{1,0:T(8,128)(2,1)S(1)} collective-permute-done((bf16[1024,256]{1,0:T(8,128)(2,1)}, bf16[1024,256]{1,0:T(8,128)(2,1)S(1)}, u32[]{:S(2)}, u32[]{:S(2)}) %collective-permute-start.4) | collective-permute-done | bytes 524320 | tf_op jit(solution)/shard_map/ppermute | solution.py:29
  79.9 1.1 constant_dynamic-update-slice_fusion.4
  81.2 8.4 %collective-permute-done.6 = bf16[1024,256]{1,0:T(8,128)(2,1)S(1)} collective-permute-done((bf16[1024,256]{1,0:T(8,128)(2,1)S(1)}, bf16[1024,256]{1,0:T(8,128)(2,1)S(1)}, u32[]{:S(2)}, u32[]{:S(2)}) %collective-permute-start.6) | collective-permute-done | bytes 524320 | tf_op jit(solution)/shard_map/ppermute | solution.py:29
  89.7 2.0 copy-done.1
  91.7 1.3 convolution_minimum_fusion
  92.9 8.6 %convolution_convert_fusion = bf16[1024,2048]{1,0:T(8,128)(2,1)} fusion(f32[1024,256]{1,0:T(8,128)S(1)} %convolution_minimum_fusion, bf16[1024,2048]{1,0:T(8,128)(2,1)} %copy-done.1, bf16[1,256,2048]{2,1,0:T(8,128)(2,1)S(1)} %copy-done, bf16[1,2048,256]{2,1,0:T(8,128)(2,1)S(1)} %copy-done.10), kind=kOutput, calls=%fused_computation.27 | convolution fusion | flops 2151940096 | bytes 11534336 | tf_op jit(solution)/shard_map/dot_general | solution.py:212
  101.5 4.4 %copy.58 = bf16[128,8,8,256]{3,2,0,1:T(8,128)(2,1)} copy(bf16[128,8,8,256]{3,2,1,0:T(8,128)(2,1)} %bitcast.128) | data formatting | bytes 8388608 | tf_op jit(solution)/shard_map/reshape | solution.py:54
  106.0 4.7 %all-to-all-start.2 = ((bf16[8,256,1024]{1,2,0:T(8,128)(2,1)}), bf16[8,256,1024]{1,2,0:T(8,128)(2,1)}, u32[]{:S(2)}, u32[]{:S(2)}) async-start(bf16[8,256,1024]{1,2,0:T(8,128)(2,1)} %bitcast.125), calls=%async_computation.2 | async-start | bytes 8388608 | tf_op jit(solution)/shard_map/all_to_all | solution.py:59
  111.7 6.5 %copy.37 = bf16[32,512,1,128]{1,3,2,0:T(8,128)(2,1)} copy(bf16[32,512,1,128]{3,1,0,2:T(8,128)(2,1)} %bitcast.127) | data formatting | bytes 8388608 | tf_op jit(solution)/shard_map/while | solution.py:167
  118.2 84.8 %while.14 = (s32[]{:T(128)}, f32[512,1,2]{0,2,1:T(2,128)S(1)}, f32[512,1,2]{0,2,1:T(2,128)S(1)}, f32[512,1,2,64]{0,3,2,1:T(8,128)S(1)}, s32[32]{0:T(128)S(1)}, /...) while((s32[]{:T(128)}, f32[512,1,2]{0,2,1:T(2,128)S(1)}, ...), condition=%wide.region_5.6_spmd, body=%wide.region_0.5_spmd.sunk | while | flops 139339264 | bytes 7965025 | solution.py:167
  120.7 3.6 %conditional.2 = ((f32[512,1,2]{0,2,1:T(2,128)S(1)}, f32[512,1,2]{0,2,1:T(2,128)S(1)}, f32[512,1,2,64]{0,3,2,1:T(8,128)S(1)})) conditional(s32[]{:T(128)} %convert_element_type.105, (f32[512,1,2]{0,2,1:T(2,128)S(1)}, f32[512,1,2]{0,2,1:T(2,128)S(1)}, f32[512,1,2,64]{0,3,2,1:T(8,128)S(1)}) %tuple.45, (s32[]{:T(128)}, s32[512]{0:T(512)S(1)}, ...), branch_computations={%region_1.1_spmd, %region_2.4_spmd} | conditional | flops 139339264 | bytes 7962702 | solution.py:164
  126.6 3.6 %conditional.2 = ((f32[512,1,2]{0,2,1:T(2,128)S(1)}, f32[512,1,2]{0,2,1:T(2,128)S(1)}, f32[512,1,2,64]{0,3,2,1:T(8,128)S(1)})) conditional(s32[]{:T(128)} %convert_element_type.105, (f32[512,1,2]{0,2,1:T(2,128)S(1)}, f32[512,1,2]{0,2,1:T(2,128)S(1)}, f32[512,1,2,64]{0,3,2,1:T(8,128)S(1)}) %tuple.45, (s32[]{:T(128)}, s32[512]{0:T(512)S(1)}, ...), branch_computations={%region_1.1_spmd, %region_2.4_spmd} | conditional | flops 139339264 | bytes 7962702 | solution.py:164
  204.2 4.7 %all-to-all-start = ((bf16[8,64,128]{2,1,0:T(8,128)(2,1)}), bf16[8,64,128]{2,1,0:T(8,128)(2,1)S(1)}, u32[]{:S(2)}, u32[]{:S(2)}) async-start(bf16[8,64,128]{2,1,0:T(8,128)(2,1)} %copy.38), calls=%async_computation | async-start | bytes 262144 | tf_op jit(solution)/shard_map/all_to_all | solution.py:177
  209.1 3.7 %reduce_sum.68 = bf16[256,1024]{0,1:T(8,128)(2,1)} reduce(bf16[8,256,1024]{1,2,0:T(8,128)(2,1)} %all-to-all-done.2, bf16[]{:T(256)} %constant.174.clone.1), dimensions={0}, to_apply=%region_12.13 | reduce | flops 1835008 | bytes 4718594 | tf_op jit(solution)/shard_map/reduce_sum | solution.py:60
  212.7 2.2 all-to-all-done
  214.9 112.4 %all-to-all-start.3 = ((bf16[256,32,32]{0,2,1:T(8,128)(2,1)}), bf16[256,32,32]{0,2,1:T(8,128)(2,1)S(1)}, u32[]{:S(2)}, u32[]{:S(2)}) async-start(bf16[256,32,32]{0,2,1:T(8,128)(2,1)} %bitcast.33), calls=%async_computation.3 | async-start | bytes 1048576 | tf_op jit(solution)/shard_map/all_to_all | solution.py:218
  327.6 3.8 %convolution_convert_fusion.1 = bf16[64,2048]{1,0:T(8,128)(2,1)} fusion(bf16[1024,2048]{1,0:T(8,128)(2,1)} %param.20, f32[1024]{0:T(1024)S(1)} %copy-done.8, f32[64]{0:T(128)S(1)} %add_rsqrt_fusion.1, bf16[8,64,128]{2,1,0:T(8,128)(2,1)S(1)} %all-to-all-done), kind=kOutput, calls=%fused_computation.28 | convolution fusion | flops 268828672 | bytes 4591872 | tf_op jit(solution)/shard_map/dot_general | solution.py:179
  331.4 12.5 %all-to-all-done.3 = bf16[256,32,32]{0,2,1:T(8,128)(2,1)S(1)} async-done(((bf16[256,32,32]{0,2,1:T(8,128)(2,1)}), bf16[256,32,32]{0,2,1:T(8,128)(2,1)S(1)}, u32[]{:S(2)}, u32[]{:S(2)}) %all-to-all-start.3) | async-done | bytes 524320 | tf_op jit(solution)/shard_map/all_to_all | solution.py:218
  344.0 1.9 gather_fusion.1
  (233 shorter events, 53.5 us)
Async XLA Ops:
  7.2 85.8 %copy-start = (bf16[1,256,2048]{2,1,0:T(8,128)(2,1)S(1)}, bf16[1,256,2048]{2,1,0:T(8,128)(2,1)}, u32[]{:S(2)}) copy-start(bf16[1,256,2048]{2,1,0:T(8,128)(2,1)} %param.27) | copy-start | bytes 3145732
  8.4 24.8 %copy-start.4 = (bf16[512,128]{1,0:T(8,128)(2,1)S(1)}, bf16[512,128]{1,0:T(8,128)(2,1)}, u32[]{:S(2)}) copy-start(bf16[512,128]{1,0:T(8,128)(2,1)} %param.17) | copy-start | bytes 393220
  21.6 28.5 %all-to-all-start.1 = ((bf16[32,32,256]{2,1,0:T(8,128)(2,1)}), bf16[32,32,256]{2,1,0:T(8,128)(2,1)S(1)}, u32[]{:S(2)}, u32[]{:S(2)}) async-start(bf16[32,32,256]{2,1,0:T(8,128)(2,1)} %broadcast_select_fusion), calls=%async_computation.1 | async-start | bytes 1048576 | tf_op jit(solution)/shard_map/all_to_all | solution.py:200
  33.2 78.5 %all-gather.4.cloned.1.call-start = ((), (), s32[]{:S(2)}) async-start(), calls=%async_computation.4 | async-start | bytes 4718592 | tf_op jit(solution)/shard_map/all_gather | solution.py:48
  50.0 9.8 %collective-permute-start = (bf16[1024,256]{1,0:T(8,128)(2,1)S(1)}, bf16[1024,256]{1,0:T(8,128)(2,1)S(1)}, u32[]{:S(2)}, u32[]{:S(2)}) collective-permute-start(bf16[1024,256]{1,0:T(8,128)(2,1)S(1)} %bitcast.129), channel_id=1, source_target_pairs={{0,1},{1,2},{2,3},{3,4},{4,5},{5,6},{6,7},{7,0},{8,9},{9,10},{10,1... | collective-permute-start | bytes 1572872 | tf_op jit(solution)/shard_map/ppermute | solution.py:29
  50.0 9.8 %collective-permute-start.1 = (bf16[1024,256]{1,0:T(8,128)(2,1)S(1)}, bf16[1024,256]{1,0:T(8,128)(2,1)S(1)}, u32[]{:S(2)}, u32[]{:S(2)}) collective-permute-start(bf16[1024,256]{1,0:T(8,128)(2,1)S(1)} %bitcast.130), channel_id=1, source_target_pairs={{0,7},{1,0},{2,1},{3,2},{4,3},{5,4},{6,5},{7,6},{8,15},{9,8},{10,9... | collective-permute-start | bytes 1572872 | tf_op jit(solution)/shard_map/ppermute | solution.py:36
  59.8 3.0 copy-start.2
  59.8 9.9 %collective-permute-start.2 = (bf16[1024,256]{1,0:T(8,128)(2,1)S(1)}, bf16[1024,256]{1,0:T(8,128)(2,1)}, u32[]{:S(2)}, u32[]{:S(2)}) collective-permute-start(bf16[1024,256]{1,0:T(8,128)(2,1)S(1)} %collective-permute-done), channel_id=1, source_target_pairs={{0,1},{1,2},{2,3},{3,4},{4,5},{5,6},{6,7},{7,0},{8,9},{9,10},{10,1... | collective-permute-start | bytes 1572872 | tf_op jit(solution)/shard_map/ppermute | solution.py:29
  59.9 10.5 %collective-permute-start.3 = (bf16[1024,256]{1,0:T(8,128)(2,1)S(1)}, bf16[1024,256]{1,0:T(8,128)(2,1)S(1)}, u32[]{:S(2)}, u32[]{:S(2)}) collective-permute-start(bf16[1024,256]{1,0:T(8,128)(2,1)S(1)} %collective-permute-done.1), channel_id=1, source_target_pairs={{0,7},{1,0},{2,1},{3,2},{4,3},{5,4},{6,5},{7,6},{8,15},{9,8},{10,9... | collective-permute-start | bytes 1572872 | tf_op jit(solution)/shard_map/ppermute | solution.py:36
  69.8 10.0 %collective-permute-start.4 = (bf16[1024,256]{1,0:T(8,128)(2,1)}, bf16[1024,256]{1,0:T(8,128)(2,1)S(1)}, u32[]{:S(2)}, u32[]{:S(2)}) collective-permute-start(bf16[1024,256]{1,0:T(8,128)(2,1)} %collective-permute-done.2), channel_id=1, source_target_pairs={{0,1},{1,2},{2,3},{3,4},{4,5},{5,6},{6,7},{7,0},{8,9},{9,10},{10,1... | collective-permute-start | bytes 1572872 | tf_op jit(solution)/shard_map/ppermute | solution.py:29
  69.8 3.6 %copy-start.3 = (bf16[1024,256]{1,0:T(8,128)(2,1)S(1)}, bf16[1024,256]{1,0:T(8,128)(2,1)}, u32[]{:S(2)}) copy-start(bf16[1024,256]{1,0:T(8,128)(2,1)} %copy-done.2) | copy-start | bytes 1572868
  70.3 21.4 %copy-start.9 = (bf16[1,2048,256]{2,1,0:T(8,128)(2,1)S(1)}, bf16[1,2048,256]{2,1,0:T(8,128)(2,1)}, u32[]{:S(2)}) copy-start(bf16[1,2048,256]{2,1,0:T(8,128)(2,1)} %param.25) | copy-start | bytes 3145732
  70.4 10.8 %collective-permute-start.5 = (bf16[1024,256]{1,0:T(8,128)(2,1)S(1)}, bf16[1024,256]{1,0:T(8,128)(2,1)S(1)}, u32[]{:S(2)}, u32[]{:S(2)}) collective-permute-start(bf16[1024,256]{1,0:T(8,128)(2,1)S(1)} %collective-permute-done.3), channel_id=1, source_target_pairs={{0,7},{1,0},{2,1},{3,2},{4,3},{5,4},{6,5},{7,6},{8,15},{9,8},{10,9... | collective-permute-start | bytes 1572872 | tf_op jit(solution)/shard_map/ppermute | solution.py:36
  79.8 9.8 %collective-permute-start.6 = (bf16[1024,256]{1,0:T(8,128)(2,1)S(1)}, bf16[1024,256]{1,0:T(8,128)(2,1)S(1)}, u32[]{:S(2)}, u32[]{:S(2)}) collective-permute-start(bf16[1024,256]{1,0:T(8,128)(2,1)S(1)} %collective-permute-done.4), channel_id=1, source_target_pairs={{0,1},{1,2},{2,3},{3,4},{4,5},{5,6},{6,7},{7,0},{8,9},{9,10},{10,1... | collective-permute-start | bytes 1572872 | tf_op jit(solution)/shard_map/ppermute | solution.py:29
  81.2 11.7 %copy-start.10 = (bf16[1,2048,256]{2,1,0:T(8,128)(2,1)S(1)}, bf16[1,2048,256]{2,1,0:T(8,128)(2,1)}, u32[]{:S(2)}) copy-start(bf16[1,2048,256]{2,1,0:T(8,128)(2,1)} %param.26) | copy-start | bytes 3145732
  89.7 2.0 copy-start.1
  106.0 4.9 %copy-start.5 = (bf16[512,128]{1,0:T(8,128)(2,1)S(1)}, bf16[512,128]{1,0:T(8,128)(2,1)}, u32[]{:S(2)}) copy-start(bf16[512,128]{1,0:T(8,128)(2,1)} %param.16) | copy-start | bytes 393220
  106.0 98.2 %all-to-all-start.2 = ((bf16[8,256,1024]{1,2,0:T(8,128)(2,1)}), bf16[8,256,1024]{1,2,0:T(8,128)(2,1)}, u32[]{:S(2)}, u32[]{:S(2)}) async-start(bf16[8,256,1024]{1,2,0:T(8,128)(2,1)} %bitcast.125), calls=%async_computation.2 | async-start | bytes 8388608 | tf_op jit(solution)/shard_map/all_to_all | solution.py:59
  118.2 90.6 %copy-start.6 = (s32[128,4]{0,1:T(4,128)S(1)}, s32[128,4]{0,1:T(4,128)}, u32[]{:S(2)}) copy-start(s32[128,4]{0,1:T(4,128)} %param.23) | copy-start | bytes 6148
  118.2 90.8 %copy-start.7 = (f32[128,4]{0,1:T(4,128)S(1)}, f32[128,4]{0,1:T(4,128)}, u32[]{:S(2)}) copy-start(f32[128,4]{0,1:T(4,128)} %param.24) | copy-start | bytes 6148
  203.1 124.6 %copy-start.8 = (f32[1024]{0:T(1024)S(1)}, f32[1024]{0:T(1024)}, u32[]{:S(2)}) copy-start(f32[1024]{0:T(1024)} %param.19) | copy-start | bytes 12292
  204.2 10.8 %all-to-all-start = ((bf16[8,64,128]{2,1,0:T(8,128)(2,1)}), bf16[8,64,128]{2,1,0:T(8,128)(2,1)S(1)}, u32[]{:S(2)}, u32[]{:S(2)}) async-start(bf16[8,64,128]{2,1,0:T(8,128)(2,1)} %copy.38), calls=%async_computation | async-start | bytes 262144 | tf_op jit(solution)/shard_map/all_to_all | solution.py:177
  214.9 129.0 %all-to-all-start.3 = ((bf16[256,32,32]{0,2,1:T(8,128)(2,1)}), bf16[256,32,32]{0,2,1:T(8,128)(2,1)S(1)}, u32[]{:S(2)}, u32[]{:S(2)}) async-start(bf16[256,32,32]{0,2,1:T(8,128)(2,1)} %bitcast.33), calls=%async_computation.3 | async-start | bytes 1048576 | tf_op jit(solution)/shard_map/all_to_all | solution.py:218
Sparse Core Ops, SparseCore 0:
  49.2 55.7 all-gather.3
